TPU v7x, 32 devices: a whole 2x2x4 slice. The times are simulated.
32 devices in a mesh: ep: 8 (over z, x), tp: 4 (over y, core).
Axes of the slice: x: 2, y: 2, z: 4, core: 2. Of those that a mesh axis runs over, the one named last changes fastest.
Arguments:
- tokens: bfloat16 [1024, 2048], P('ep'), may hold values from -6 to 6
- norm_gain: float32 [2048], replicated, may hold values from 0.1 to 1.9
- expert_ids: int32 [1024, 2], P('ep'), may hold values from 0 to 7, all different within a row; in each aligned block of 128 rows (0 to 127, 128 to 255, ...) at most 64 rows name the same one
- route_weights: float32 [1024, 2], P('ep'), may hold values from 0.2 to 1
- w_gate: bfloat16 [8, 2048, 4096], P('ep', None, 'tp'), may hold values from -0.125 to 0.125
- w_up: bfloat16 [8, 2048, 4096], P('ep', None, 'tp'), may hold values from -0.125 to 0.125
- w_down: bfloat16 [8, 4096, 2048], P('ep', 'tp'), may hold values from -0.09375 to 0.09375
Outputs:
- combined: bfloat16 [1024, 2048], P('ep', 'tp')
Inputs may be any that keep to these rules, and one draw needn't show every extreme that they name: `expert_ids`: each row names two different experts; among the rows of one device no expert is named more than 64 times, and in every draw some expert is named exactly 64 times there.
All inputs are finite; a program needn't handle non-finite values.
Results may differ from a plain program's by a relative error of at most 0.019.
Values may be sent and summed in bfloat16 or wider, within the bound.
A program may use at most 64 MiB of HBM per device.

v0:
```python
import jax
import jax.numpy as jnp
from jax import lax
from jax.sharding import PartitionSpec as P

epsilon = 1e-06


def per_device(tokens, norm_gain, expert_ids, route_weights, w_gate, w_up, w_down):
    tok_rows, model_width = tokens.shape
    local_count = w_gate.shape[0]
    experts = local_count * lax.axis_size("ep")
    rank_count = lax.axis_size("tp")
    column_width = model_width // rank_count
    capacity = 4 * tok_rows // experts
    as_float = tokens.astype(jnp.float32)
    scale = lax.rsqrt(jnp.mean(as_float * as_float, axis=-1, keepdims=True) + epsilon)
    normed = (as_float * scale * norm_gain[None, :]).astype(jnp.bfloat16)
    flat_ids = expert_ids.reshape(-1)
    one_hot = (flat_ids[:, None] == jnp.arange(experts, dtype=jnp.int32)[None, :]).astype(jnp.int32)
    slot_index = jnp.sum((jnp.cumsum(one_hot, axis=0) - one_hot) * one_hot, axis=1)
    target = flat_ids * capacity + slot_index
    token_rows = jnp.repeat(normed, 2, axis=0)
    token_rows = lax.dynamic_slice_in_dim(
        token_rows, lax.axis_index("tp") * column_width, column_width, 1
    )
    outgoing = (
        jnp.zeros((experts * capacity, token_rows.shape[1]), jnp.bfloat16)
        .at[target]
        .set(token_rows)
    )
    outgoing = outgoing.reshape(experts, capacity, token_rows.shape[1])
    arrived = lax.all_to_all(outgoing, "ep", split_axis=0, concat_axis=1, tiled=True)
    piece = lax.all_gather(arrived, "tp", axis=2, tiled=True)
    gate_part = jnp.einsum("erd,edf->erf", piece, w_gate, preferred_element_type=jnp.float32)
    up_part = jnp.einsum("erd,edf->erf", piece, w_up, preferred_element_type=jnp.float32)
    hidden = (jax.nn.silu(gate_part) * up_part).astype(jnp.bfloat16)
    partial_value = jnp.einsum("erf,efd->erd", hidden, w_down, preferred_element_type=jnp.float32)
    summed = lax.psum_scatter(
        partial_value.astype(jnp.bfloat16), "tp", scatter_dimension=2, tiled=True
    )
    returned = lax.all_to_all(summed, "ep", split_axis=1, concat_axis=0, tiled=True)
    picked = returned.reshape(experts * capacity, column_width)[target]
    picked = picked.reshape(tok_rows, 2, column_width).astype(jnp.float32)
    return jnp.sum(picked * route_weights[:, :, None], axis=1).astype(jnp.bfloat16)


def solution(mesh):
    in_specs = (
        P("ep", None),
        P(),
        P("ep", None),
        P("ep", None),
        P("ep", None, "tp"),
        P("ep", None, "tp"),
        P("ep", "tp", None),
    )
    out_specs = P("ep", "tp")
    return jax.shard_map(
        per_device, mesh=mesh, in_specs=in_specs, out_specs=out_specs, check_vma=False
    )
```

profile of v0, /device:TPU:0, one launch (start us, length us, event | category | flops | bytes accessed | tf_op | source)
XLA Modules:
  0.0 143.9 jit_solution(12117852993632384072)
XLA Ops:
  6.5 0.8 copy.19
  7.3 0.1 eq.29
  7.5 0.1 eq.25
  7.6 0.7 broadcast_multiply_fusion
  8.3 0.6 reduce-window.6
  8.9 0.2 slice_reduce_fusion
  9.1 0.1 copy.18
  9.2 0.1 mul.60
  9.4 1.2 fusion.18
  10.6 1.2 fusion.20
  11.9 0.6 broadcast_in_dim.5
  12.5 0.4 reshape.102
  12.9 0.1 fusion.29
  13.0 1.7 %scatter_custom_fusion = bf16[512,512]{1,0:T(8,128)(2,1)S(1)} fusion(s32[256]{0:T(256)S(1)} %bitcast.52, bf16[256,2048]{1,0:T(8,128)(2,1)S(1)} %reshape.102, s32[]{:T(128)} %constant.12.clone.1, s32[]{:T(128)S(6)} %select_n.15, bf16[]{:T(256)} %constant.10.clone.1), kind=kCustom, calls=%fused_computation.20 | custom fusion | bytes 786442 | tf_op jit(solution)/shard_map/scatter | solution.py:30
  14.7 21.7 %all_to_all.21 = bf16[8,64,512]{2,1,0:T(8,128)(2,1)} all-to-all(bf16[8,64,512]{2,1,0:T(8,128)(2,1)S(1)} %bitcast.51), channel_id=1, replica_groups=mesh['ep'=8,'tp'=4] {'ep'}, dimensions={0} | all-to-all | bytes 1048576 | tf_op jit(solution)/shard_map/all_to_all | solution.py:33
  36.5 0.2 reduce-scatter.2.cloned.1.call-start
  36.7 21.5 %all-gather.2.cloned.1.call-done = bf16[1,512,2048]{2,1,0:T(8,128)(2,1)} async-done(((bf16[1,512,512]{2,1,0:T(8,128)(2,1)}), bf16[1,512,2048]{2,1,0:T(8,128)(2,1)}) %all-gather.2.cloned.1.call-update) | async-done | bytes 2097168 | tf_op jit(solution)/shard_map/all_gather | solution.py:34
  58.2 6.6 %fusion.4 = f32[512,1024]{1,0:T(8,128)} fusion(bf16[1,2048,1024]{2,1,0:T(8,128)(2,1)} %param.11, bf16[1,512,2048]{2,1,0:T(8,128)(2,1)} %all-gather.2.cloned.1.call-done), kind=kOutput, calls=%fused_computation.6 | convolution fusion | flops 2147483648 | bytes 8388608 | tf_op jit(solution)/shard_map/erd,edf->erf/dot_general | solution.py:35
  64.8 10.0 %fusion.9 = bf16[1,512,2048]{2,1,0:T(8,128)(2,1)} fusion(bf16[1,1024,2048]{2,1,0:T(8,128)(2,1)} %param.13, f32[512,1024]{1,0:T(8,128)} %fusion.4, bf16[1,2048,1024]{2,1,0:T(8,128)(2,1)} %param.12, bf16[1,512,2048]{2,1,0:T(8,128)(2,1)S(1)} %copy-done.1), kind=kOutput, calls=%fused_computation.9 | convolution fusion | flops 4299161600 | bytes 14680064 | tf_op jit(solution)/shard_map/erf,efd->erd/dot_general | solution.py:38
  74.8 31.3 %reduce-scatter.2.cloned.1.call-done = bf16[1,512,512]{2,1,0:T(8,128)(2,1)} async-done(((bf16[1,512,2048]{2,1,0:T(8,128)(2,1)}), bf16[1,512,512]{2,1,0:T(8,128)(2,1)}) %reduce-scatter.2.cloned.1.call-update) | async-done | bytes 524304 | tf_op jit(solution)/shard_map/reduce_scatter | solution.py:39
  106.2 1.9 %copy.27 = bf16[1,512,512]{2,0,1:T(2,128)(2,1)S(1)} copy(bf16[1,512,512]{2,1,0:T(8,128)(2,1)} %reduce-scatter.2.cloned.1.call-done) | data formatting | bytes 1048576 | tf_op jit(solution)/shard_map/reduce_scatter | solution.py:39
  108.0 0.5 broadcast.73
  108.5 4.0 %reduce.2 = bf16[512,512]{1,0:T(8,128)(2,1)S(1)} reduce(bf16[512,1,512]{2,1,0:T(2,128)(2,1)S(1)} %bitcast.49, bf16[]{:T(256)} %broadcast.73), dimensions={1}, to_apply=%bitcast.46.reduce_sub_computation | reduce | bytes 1048578
  112.5 1.2 reshape.129
  113.7 5.5 %all-to-all-start.1 = ((bf16[8,2,16384]{2,1,0:T(2,128)(2,1)}), bf16[8,2,16384]{2,1,0:T(2,128)(2,1)S(1)}, u32[]{:S(2)}, u32[]{:S(2)}) async-start(bf16[8,2,16384]{2,1,0:T(2,128)(2,1)} %reshape.129), calls=%async_computation.2 | async-start | bytes 1048576 | tf_op jit(solution)/shard_map/all_to_all | solution.py:42
  119.2 0.1 copy.22
  119.3 14.2 %all-to-all-done.1 = bf16[8,2,16384]{2,1,0:T(2,128)(2,1)S(1)} async-done(((bf16[8,2,16384]{2,1,0:T(2,128)(2,1)}), bf16[8,2,16384]{2,1,0:T(2,128)(2,1)S(1)}, u32[]{:S(2)}, u32[]{:S(2)}) %all-to-all-start.1) | async-done | bytes 524320 | tf_op jit(solution)/shard_map/all_to_all | solution.py:42
  133.5 0.5 reshape.130
  134.0 0.1 copy.26
  134.2 1.2 gather_fusion
  135.3 0.3 reshape.109
  135.7 1.4 multiply_reduce_fusion
  (13 shorter events, 0.1 us)
Async XLA Ops:
  6.5 51.7 %all-gather.2.cloned.1.call-start = ((), (), s32[]{:S(2)}) async-start(), calls=%async_computation.3 | async-start | bytes 2621440 | tf_op jit(solution)/shard_map/all_gather | solution.py:34
  36.5 69.7 %reduce-scatter.2.cloned.1.call-start = ((), (), s32[]{:S(2)}) async-start(), calls=%async_computation.4 | async-start | bytes 2621440 | tf_op jit(solution)/shard_map/reduce_scatter | solution.py:39
  58.2 6.6 %copy-start.1 = (bf16[1,512,2048]{2,1,0:T(8,128)(2,1)S(1)}, bf16[1,512,2048]{2,1,0:T(8,128)(2,1)}, u32[]{:S(2)}) copy-start(bf16[1,512,2048]{2,1,0:T(8,128)(2,1)} %all-gather.2.cloned.1.call-done) | copy-start | bytes 6291460
  108.0 11.2 %copy-start = (f32[128,2]{0,1:T(2,128)S(1)}, f32[128,2]{0,1:T(2,128)}, u32[]{:S(2)}) copy-start(f32[128,2]{0,1:T(2,128)} %param.10) | copy-start | bytes 3076
  113.7 19.8 %all-to-all-start.1 = ((bf16[8,2,16384]{2,1,0:T(2,128)(2,1)}), bf16[8,2,16384]{2,1,0:T(2,128)(2,1)S(1)}, u32[]{:S(2)}, u32[]{:S(2)}) async-start(bf16[8,2,16384]{2,1,0:T(2,128)(2,1)} %reshape.129), calls=%async_computation.2 | async-start | bytes 1048576 | tf_op jit(solution)/shard_map/all_to_all | solution.py:42
Sparse Core Ops, SparseCore 0:
  36.6 21.5 all-gather.1
  75.0 31.1 reduce-scatter.1
where the time goes:
time: 144 us
  waiting for transfers between devices  67.1 us (47%)
  blocking collectives  21.7 us (15%)
  matrix products  16.6 us (12%)
  between operations  13.5 us (9%)
  local copies, waits for them, and re-layouts  10.1 us (7%)
  other arithmetic  9.19 us (6%)
  starting transfers between devices  5.74 us (4%)
    reduce_scatter x1, waiting for transfers between devices, per_device(): lax.psum_scatter(partial_value.astype(jnp.bfloat16), 'tp', scatter_dimens...  31.3 us
    all_to_all x1, blocking collectives, per_device(): lax.all_to_all(outgoing, 'ep', split_axis=0, concat_axis=1, tiled=True)  21.7 us
    all_gather x1, waiting for transfers between devices, per_device(): piece = lax.all_gather(arrived, 'tp', axis=2, tiled=True)  21.5 us
    all_to_all x1, waiting for transfers between devices, per_device(): lax.all_to_all(summed, 'ep', split_axis=1, concat_axis=0, tiled=True)  14.2 us
    dot_general x1, matrix products, per_device(): jnp.einsum('erf,efd->erd', hidden, w_down, preferred_element_type=jnp.flo...  9.99 us
    dot_general x1, matrix products, per_device(): jnp.einsum('erd,edf->erf', piece, w_gate, preferred_element_type=jnp.floa...  6.59 us
    all_to_all x1, starting transfers between devices, per_device(): lax.all_to_all(summed, 'ep', split_axis=1, concat_axis=0, tiled=True)  5.51 us
    unnamed x1, other arithmetic  3.95 us
  transfers between devices with their start and end apart: 3, of which 3 were waited for; matrix products, arithmetic and copies ran while one was open for 0% of the time, Pallas kernels for 0%

commit v1 on v0

--- a/solution.py
+++ b/solution.py
@@ -4,6 +4,12 @@
 from jax.sharding import PartitionSpec as P
 
 epsilon = 1e-06
+
+
+def stack_and_merge(x, mesh_axis, dim):
+    blocks = lax.all_gather(x, mesh_axis, axis=0, tiled=False)
+    whole = jnp.concatenate(blocks, axis=dim)
+    return whole
 
 
 def per_device(tokens, norm_gain, expert_ids, route_weights, w_gate, w_up, w_down):
@@ -31,7 +37,7 @@
     )
     outgoing = outgoing.reshape(experts, capacity, token_rows.shape[1])
     arrived = lax.all_to_all(outgoing, "ep", split_axis=0, concat_axis=1, tiled=True)
-    piece = lax.all_gather(arrived, "tp", axis=2, tiled=True)
+    piece = stack_and_merge(arrived, "tp", 2)
     gate_part = jnp.einsum("erd,edf->erf", piece, w_gate, preferred_element_type=jnp.float32)
     up_part = jnp.einsum("erd,edf->erf", piece, w_up, preferred_element_type=jnp.float32)
     hidden = (jax.nn.silu(gate_part) * up_part).astype(jnp.bfloat16)

time: 144 us -> 147 us (1.021)
  local copies, waits for them, and re-layouts: 10.1 us -> 12.8 us
    all_gather x0 -> x1, local copies, waits for them, and re-layouts: none -> 2.79 us  [stack_and_merge(): blocks = lax.all_gather(x, mesh_axis, axis=0, tiled=False)]
    unnamed x10 -> x8, local copies, waits for them, and re-layouts: 3.23 us -> 3.23 us
where the time goes in v1:
time: 147 us; the launch traced here: 146 us
  waiting for transfers between devices  67.1 us (46%)
  blocking collectives  21.7 us (15%)
  matrix products  16.1 us (11%)
  between operations  13.5 us (9%)
  local copies, waits for them, and re-layouts  12.8 us (9%)
  other arithmetic  9.19 us (6%)
  starting transfers between devices  5.74 us (4%)
    reduce_scatter x1, waiting for transfers between devices, per_device(): lax.psum_scatter(partial_value.astype(jnp.bfloat16), 'tp', scatter_dimens...  31.3 us
    all_to_all x1, blocking collectives, per_device(): lax.all_to_all(outgoing, 'ep', split_axis=0, concat_axis=1, tiled=True)  21.7 us
    all_gather x1, waiting for transfers between devices, stack_and_merge(): blocks = lax.all_gather(x, mesh_axis, axis=0, tiled=False)  21.5 us
    all_to_all x1, waiting for transfers between devices, per_device(): lax.all_to_all(summed, 'ep', split_axis=1, concat_axis=0, tiled=True)  14.2 us
    dot_general x1, matrix products, per_device(): jnp.einsum('erf,efd->erd', hidden, w_down, preferred_element_type=jnp.flo...  10.2 us
    dot_general x1, matrix products, per_device(): jnp.einsum('erd,edf->erf', piece, w_gate, preferred_element_type=jnp.floa...  5.88 us
    all_to_all x1, starting transfers between devices, per_device(): lax.all_to_all(summed, 'ep', split_axis=1, concat_axis=0, tiled=True)  5.51 us
    unnamed x1, other arithmetic  3.95 us
  transfers between devices with their start and end apart: 3, of which 3 were waited for; matrix products, arithmetic and copies ran while one was open for 0% of the time, Pallas kernels for 0%

profile of v1, /device:TPU:0, one launch (start us, length us, event | category | flops | bytes accessed | tf_op | source)
XLA Modules:
  0.0 146.1 jit_solution(932356380528511212)
XLA Ops:
  6.5 0.8 copy.26
  7.3 0.1 eq.29
  7.5 0.1 eq.25
  7.6 0.7 broadcast_multiply_fusion
  8.3 0.6 reduce-window.6
  8.9 0.2 slice_reduce_fusion
  9.1 0.1 copy.25
  9.2 0.1 mul.60
  9.4 1.2 fusion.14
  10.6 1.2 fusion.16
  11.9 0.6 broadcast_in_dim.5
  12.5 0.4 reshape.109
  13.0 1.7 %scatter_custom_fusion = bf16[512,512]{1,0:T(8,128)(2,1)S(1)} fusion(s32[256]{0:T(256)S(1)} %bitcast.50, bf16[256,2048]{1,0:T(8,128)(2,1)S(1)} %reshape.109, s32[]{:T(128)} %constant.12.clone.1, s32[]{:T(128)S(6)} %select_n.15, bf16[]{:T(256)} %constant.10.clone.1), kind=kCustom, calls=%fused_computation.18 | custom fusion | bytes 786442 | tf_op jit(solution)/shard_map/scatter | solution.py:36
  14.7 21.7 %all_to_all.8 = bf16[8,64,512]{2,1,0:T(8,128)(2,1)} all-to-all(bf16[8,64,512]{2,1,0:T(8,128)(2,1)S(1)} %bitcast.49), channel_id=1, replica_groups=mesh['ep'=8,'tp'=4] {'ep'}, dimensions={0} | all-to-all | bytes 1048576 | tf_op jit(solution)/shard_map/all_to_all | solution.py:39
  36.5 0.2 reduce-scatter.2.cloned.1.call-start
  36.7 21.5 %all-gather.2.cloned.1.call-done = bf16[4,1,512,512]{3,2,1,0:T(8,128)(2,1)} async-done(((bf16[1,1,512,512]{3,2,1,0:T(8,128)(2,1)}), bf16[4,1,512,512]{3,2,1,0:T(8,128)(2,1)}) %all-gather.2.cloned.1.call-update) | async-done | bytes 2097168 | tf_op jit(solution)/shard_map/all_gather | solution.py:10
  58.2 2.8 %copy.28 = bf16[4,1,512,512]{2,3,0,1:T(8,128)(2,1)S(1)} copy(bf16[4,1,512,512]{3,2,1,0:T(8,128)(2,1)} %all-gather.2.cloned.1.call-done) | data formatting | bytes 4194304 | tf_op jit(solution)/shard_map/all_gather | solution.py:10
  61.0 5.9 %fusion.4 = f32[512,1024]{1,0:T(8,128)} fusion(bf16[512,2048]{0,1:T(8,128)(2,1)S(1)} %bitcast.46, bf16[1,2048,1024]{2,1,0:T(8,128)(2,1)} %param.11), kind=kOutput, calls=%fused_computation.6 | convolution fusion | flops 2147483648 | bytes 8388608 | tf_op jit(solution)/shard_map/erd,edf->erf/dot_general | solution.py:41
  66.9 10.2 %fusion.9 = bf16[1,512,2048]{2,1,0:T(8,128)(2,1)} fusion(bf16[1,1024,2048]{2,1,0:T(8,128)(2,1)} %param.13, f32[512,1024]{1,0:T(8,128)} %fusion.4, bf16[512,2048]{0,1:T(8,128)(2,1)S(1)} %bitcast.47, bf16[1,2048,1024]{2,1,0:T(8,128)(2,1)} %param.12), kind=kOutput, calls=%fused_computation.9 | convolution fusion | flops 4299161600 | bytes 14680064 | tf_op jit(solution)/shard_map/erf,efd->erd/dot_general | solution.py:44
  77.1 31.3 %reduce-scatter.2.cloned.1.call-done = bf16[1,512,512]{2,1,0:T(8,128)(2,1)} async-done(((bf16[1,512,2048]{2,1,0:T(8,128)(2,1)}), bf16[1,512,512]{2,1,0:T(8,128)(2,1)}) %reduce-scatter.2.cloned.1.call-update) | async-done | bytes 524304 | tf_op jit(solution)/shard_map/reduce_scatter | solution.py:45
  108.4 1.9 %copy.35 = bf16[1,512,512]{2,0,1:T(2,128)(2,1)S(1)} copy(bf16[1,512,512]{2,1,0:T(8,128)(2,1)} %reduce-scatter.2.cloned.1.call-done) | data formatting | bytes 1048576 | tf_op jit(solution)/shard_map/reduce_scatter | solution.py:45
  110.3 0.5 broadcast.73
  110.8 4.0 %reduce.2 = bf16[512,512]{1,0:T(8,128)(2,1)S(1)} reduce(bf16[512,1,512]{2,1,0:T(2,128)(2,1)S(1)} %bitcast.45, bf16[]{:T(256)} %broadcast.73), dimensions={1}, to_apply=%bitcast.42.reduce_sub_computation | reduce | bytes 1048578
  114.8 1.2 reshape.137
  115.9 5.5 %all-to-all-start.1 = ((bf16[8,2,16384]{2,1,0:T(2,128)(2,1)}), bf16[8,2,16384]{2,1,0:T(2,128)(2,1)S(1)}, u32[]{:S(2)}, u32[]{:S(2)}) async-start(bf16[8,2,16384]{2,1,0:T(2,128)(2,1)} %reshape.137), calls=%async_computation.2 | async-start | bytes 1048576 | tf_op jit(solution)/shard_map/all_to_all | solution.py:48
  121.4 0.1 copy.30
  121.6 14.2 %all-to-all-done.1 = bf16[8,2,16384]{2,1,0:T(2,128)(2,1)S(1)} async-done(((bf16[8,2,16384]{2,1,0:T(2,128)(2,1)}), bf16[8,2,16384]{2,1,0:T(2,128)(2,1)S(1)}, u32[]{:S(2)}, u32[]{:S(2)}) %all-to-all-start.1) | async-done | bytes 524320 | tf_op jit(solution)/shard_map/all_to_all | solution.py:48
  135.7 0.5 reshape.138
  136.3 0.1 copy.34
  136.4 1.2 gather_fusion
  137.6 0.3 reshape.117
  137.9 1.4 multiply_reduce_fusion
  (12 shorter events, 0.2 us)
Async XLA Ops:
  6.5 51.7 %all-gather.2.cloned.1.call-start = ((), (), s32[]{:S(2)}) async-start(), calls=%async_computation.3 | async-start | bytes 2621440 | tf_op jit(solution)/shard_map/all_gather | solution.py:10
  36.5 72.0 %reduce-scatter.2.cloned.1.call-start = ((), (), s32[]{:S(2)}) async-start(), calls=%async_computation.4 | async-start | bytes 2621440 | tf_op jit(solution)/shard_map/reduce_scatter | solution.py:45
  110.3 11.2 %copy-start = (f32[128,2]{0,1:T(2,128)S(1)}, f32[128,2]{0,1:T(2,128)}, u32[]{:S(2)}) copy-start(f32[128,2]{0,1:T(2,128)} %param.10) | copy-start | bytes 3076
  115.9 19.8 %all-to-all-start.1 = ((bf16[8,2,16384]{2,1,0:T(2,128)(2,1)}), bf16[8,2,16384]{2,1,0:T(2,128)(2,1)S(1)}, u32[]{:S(2)}, u32[]{:S(2)}) async-start(bf16[8,2,16384]{2,1,0:T(2,128)(2,1)} %reshape.137), calls=%async_computation.2 | async-start | bytes 1048576 | tf_op jit(solution)/shard_map/all_to_all | solution.py:48
Sparse Core Ops, SparseCore 0:
  36.6 21.5 all-gather.1
  77.2 31.1 reduce-scatter.1
